TPU v7x, 32 devices: a whole 2x2x4 slice. The times are simulated.
32 devices in a mesh: sp: 8 (over z, y), tp: 4 (over x, core).
Axes of the slice: x: 2, y: 2, z: 4, core: 2. Of those that a mesh axis runs over, the one named last changes fastest.
Arguments:
- tokens: bfloat16 [6, 2048, 2048], P(None, 'sp', 'tp'), may hold values from -6 to 6
- norm_gains: float32 [3, 2048], replicated, may hold values from 0.5 to 1.5
- weight_outer: bfloat16 [3, 2048, 1024], P(None, 'sp', 'tp'), may hold values from -0.125 to 0.125
- weight_inner: bfloat16 [3, 2048, 1024], P(None, 'sp', 'tp'), may hold values from -0.125 to 0.125
- weight_value: bfloat16 [3, 2048, 1024], P(None, 'sp', 'tp'), may hold values from -0.125 to 0.125
- conv_taps: bfloat16 [3, 3, 1024], P(None, None, 'tp'), may hold values from -3.5 to 3.5
- weight_output: bfloat16 [3, 1024, 2048], P(None, 'sp', 'tp'), may hold values from -0.1875 to 0.1875
Outputs:
- mixed_out: float32 [6, 2048, 2048], P(None, 'sp', 'tp')
All inputs are finite; a program needn't handle non-finite values.
Results may differ from a plain program's by a relative error of at most 0.03.
Values may be sent and summed in bfloat16 or wider, within the bound.
A program may use at most 128 MiB of HBM per device.

v0:
```python
import jax
import jax.numpy as jnp
from jax import lax
from jax.sharding import PartitionSpec as P

epsilon = 1e-06


def taken_in(array, axis, dim, take_in, carry):
    whole = jax.tree.map(lambda part: lax.all_gather(part, axis, axis=dim, tiled=True), array)
    return take_in(carry, whole, jnp.int32(0))


def from_behind(block, axis, distance):
    devices = range(lax.axis_size(axis))
    route = [(i - distance, i) for i in devices if i - distance in devices]
    return lax.ppermute(block, axis, route)


def normalize(values_in, gain_row):
    values = values_in.astype(jnp.float32)
    scale = lax.rsqrt(jnp.mean(values * values, axis=-1, keepdims=True) + epsilon)
    return (values * scale * gain_row.astype(jnp.float32)).astype(jnp.bfloat16)


def convolve(extended, taps):
    width = taps.shape[0]
    out_rows = extended.shape[1] - (width - 1)
    total = jnp.zeros((extended.shape[0], out_rows, extended.shape[2]), jnp.float32)
    for offset in range(width):
        total = total + taps[offset].astype(jnp.float32) * extended[:, offset : offset + out_rows]
    return total


def project_input(normed, pieces_in):
    empty = jnp.zeros((normed.shape[0], pieces_in[0].shape[1]), jnp.float32)

    def add_rows(totals, pieces, start):
        columns = lax.dynamic_slice_in_dim(normed, start, pieces[0].shape[0], 1)
        return tuple(
            (
                total + jnp.dot(columns, piece, preferred_element_type=jnp.float32)
                for total, piece in zip(totals, pieces)
            )
        )

    return taken_in(
        (pieces_in[0], pieces_in[1], pieces_in[2]), "sp", 0, add_rows, (empty, empty, empty)
    )


def project_output(flat_mix, piece_in):
    empty = jnp.zeros((flat_mix.shape[0], piece_in.shape[1]), jnp.float32)

    def add_rows(total, piece, start):
        columns = lax.dynamic_slice_in_dim(flat_mix, start, piece.shape[0], 1)
        return total + jnp.dot(columns, piece, preferred_element_type=jnp.float32)

    return taken_in(piece_in, "sp", 0, add_rows, empty)


def local(tokens, norm_gains, weight_outer, weight_inner, weight_value, conv_taps, weight_output):
    layers = conv_taps.shape[0]
    history = conv_taps.shape[1] - 1
    sequences = tokens.shape[0]
    current = tokens
    result = None
    for layer in range(layers):
        rows = current.shape[1]
        whole = lax.all_gather(current, "tp", axis=2, tiled=True)
        normed = normalize(whole, norm_gains[layer]).reshape(sequences * rows, whole.shape[2])
        outer, inner, value = project_input(
            normed, (weight_outer[layer], weight_inner[layer], weight_value[layer])
        )
        outer = outer.astype(jnp.bfloat16)
        inner = inner.astype(jnp.bfloat16)
        value = value.astype(jnp.bfloat16)
        outer, inner, value = lax.optimization_barrier((outer, inner, value))
        channels = outer.shape[1]
        outer = outer.reshape(sequences, rows, channels)
        gated = (inner.astype(jnp.float32) * value.astype(jnp.float32)).reshape(
            sequences, rows, channels
        )
        earlier = from_behind(gated[:, rows - history :], "sp", 1)
        extended = jnp.concatenate([earlier, gated], axis=1)
        kept = outer
        conved = convolve(extended, conv_taps[layer])
        mixer = (kept.astype(jnp.float32) * conved).astype(jnp.bfloat16)
        out_rows = mixer.shape[1]
        full_mix = lax.all_gather(mixer, "tp", axis=2, tiled=True)
        flat_mix = full_mix.reshape(sequences * out_rows, full_mix.shape[2])
        projected = project_output(flat_mix, weight_output[layer])
        result = projected.reshape(sequences, out_rows, projected.shape[1])
        current = result.astype(jnp.bfloat16)
    return result


def solution(mesh):
    placed = (
        P(None, "sp", "tp"),
        P(),
        P(None, "sp", "tp"),
        P(None, "sp", "tp"),
        P(None, "sp", "tp"),
        P(None, None, "tp"),
        P(None, "sp", "tp"),
    )
    return jax.shard_map(
        local, mesh=mesh, in_specs=placed, out_specs=P(None, "sp", "tp"), check_vma=False
    )
```

profile of v0, /device:TPU:0, one launch (start us, length us, event | category | flops | bytes accessed | tf_op | source)
XLA Modules:
  0.0 757.6 jit_solution(11629076176349233693)
XLA Ops:
  10.9 47.1 %all-gather.31.cloned.1.call-done = bf16[6,256,2048]{2,1,0:T(8,128)(2,1)} async-done(((bf16[6,256,512]{2,1,0:T(8,128)(2,1)}), bf16[6,256,2048]{2,1,0:T(8,128)(2,1)}) %all-gather.31.cloned.1.call-update) | async-done | bytes 6291472 | tf_op jit(solution)/shard_map/all_gather | solution.py:70
  66.8 33.7 %all-gather.47.cloned.1.call-done = bf16[1,2048,256]{2,1,0:T(8,128)(2,1)} async-done(((bf16[1,256,256]{2,1,0:T(8,128)(2,1)}), bf16[1,2048,256]{2,1,0:T(8,128)(2,1)}) %all-gather.47.cloned.1.call-update) | async-done | bytes 1048592 | tf_op jit(solution)/shard_map/all_gather | solution.py:10
  105.3 36.3 %all-gather.45.cloned.1.call-done = bf16[1,2048,256]{2,1,0:T(8,128)(2,1)} async-done(((bf16[1,256,256]{2,1,0:T(8,128)(2,1)}), bf16[1,2048,256]{2,1,0:T(8,128)(2,1)}) %all-gather.45.cloned.1.call-update) | async-done | bytes 1048592 | tf_op jit(solution)/shard_map/all_gather | solution.py:10
  141.6 4.9 convolution_convert_fusion.7
  146.5 36.1 %all-gather.43.cloned.1.call-done = bf16[1,2048,256]{2,1,0:T(8,128)(2,1)} async-done(((bf16[1,256,256]{2,1,0:T(8,128)(2,1)}), bf16[1,2048,256]{2,1,0:T(8,128)(2,1)}) %all-gather.43.cloned.1.call-update) | async-done | bytes 1048592 | tf_op jit(solution)/shard_map/all_gather | solution.py:10
  193.1 30.5 %all-gather.49.cloned.1.call-done = bf16[1,1024,512]{2,1,0:T(8,128)(2,1)} async-done(((bf16[1,128,512]{2,1,0:T(8,128)(2,1)}), bf16[1,1024,512]{2,1,0:T(8,128)(2,1)}) %all-gather.49.cloned.1.call-update) | async-done | bytes 1048592 | tf_op jit(solution)/shard_map/all_gather | solution.py:10
  223.6 29.1 %all-gather.33.cloned.1.call-done = bf16[6,256,1024]{2,1,0:T(8,128)(2,1)} async-done(((bf16[6,256,256]{2,1,0:T(8,128)(2,1)}), bf16[6,256,1024]{2,1,0:T(8,128)(2,1)}) %all-gather.33.cloned.1.call-update) | async-done | bytes 3145744 | tf_op jit(solution)/shard_map/all_gather | solution.py:90
  252.7 5.1 convolution_convert_fusion.10
  260.8 43.5 %all-gather.35.cloned.1.call-done = bf16[6,256,2048]{2,1,0:T(8,128)(2,1)} async-done(((bf16[6,256,512]{2,1,0:T(8,128)(2,1)}), bf16[6,256,2048]{2,1,0:T(8,128)(2,1)}) %all-gather.35.cloned.1.call-update) | async-done | bytes 6291472 | tf_op jit(solution)/shard_map/all_gather | solution.py:70
  313.1 33.7 %all-gather.55.cloned.1.call-done = bf16[1,2048,256]{2,1,0:T(8,128)(2,1)} async-done(((bf16[1,256,256]{2,1,0:T(8,128)(2,1)}), bf16[1,2048,256]{2,1,0:T(8,128)(2,1)}) %all-gather.55.cloned.1.call-update) | async-done | bytes 1048592 | tf_op jit(solution)/shard_map/all_gather | solution.py:10
  351.6 36.3 %all-gather.53.cloned.1.call-done = bf16[1,2048,256]{2,1,0:T(8,128)(2,1)} async-done(((bf16[1,256,256]{2,1,0:T(8,128)(2,1)}), bf16[1,2048,256]{2,1,0:T(8,128)(2,1)}) %all-gather.53.cloned.1.call-update) | async-done | bytes 1048592 | tf_op jit(solution)/shard_map/all_gather | solution.py:10
  392.7 36.2 %all-gather.51.cloned.1.call-done = bf16[1,2048,256]{2,1,0:T(8,128)(2,1)} async-done(((bf16[1,256,256]{2,1,0:T(8,128)(2,1)}), bf16[1,2048,256]{2,1,0:T(8,128)(2,1)}) %all-gather.51.cloned.1.call-update) | async-done | bytes 1048592 | tf_op jit(solution)/shard_map/all_gather | solution.py:10
  428.9 4.9 convolution_convert_fusion.5
  439.4 30.6 %all-gather.57.cloned.1.call-done = bf16[1,1024,512]{2,1,0:T(8,128)(2,1)} async-done(((bf16[1,128,512]{2,1,0:T(8,128)(2,1)}), bf16[1,1024,512]{2,1,0:T(8,128)(2,1)}) %all-gather.57.cloned.1.call-update) | async-done | bytes 1048592 | tf_op jit(solution)/shard_map/all_gather | solution.py:10
  470.0 29.1 %all-gather.37.cloned.1.call-done = bf16[6,256,1024]{2,1,0:T(8,128)(2,1)} async-done(((bf16[6,256,256]{2,1,0:T(8,128)(2,1)}), bf16[6,256,1024]{2,1,0:T(8,128)(2,1)}) %all-gather.37.cloned.1.call-update) | async-done | bytes 3145744 | tf_op jit(solution)/shard_map/all_gather | solution.py:90
  499.1 5.1 convolution_convert_fusion.9
  506.8 43.9 %all-gather.39.cloned.1.call-done = bf16[6,256,2048]{2,1,0:T(8,128)(2,1)} async-done(((bf16[6,256,512]{2,1,0:T(8,128)(2,1)}), bf16[6,256,2048]{2,1,0:T(8,128)(2,1)}) %all-gather.39.cloned.1.call-update) | async-done | bytes 6291472 | tf_op jit(solution)/shard_map/all_gather | solution.py:70
  559.5 33.5 %all-gather.63.cloned.1.call-done = bf16[1,2048,256]{2,1,0:T(8,128)(2,1)} async-done(((bf16[1,256,256]{2,1,0:T(8,128)(2,1)}), bf16[1,2048,256]{2,1,0:T(8,128)(2,1)}) %all-gather.63.cloned.1.call-update) | async-done | bytes 1048592 | tf_op jit(solution)/shard_map/all_gather | solution.py:10
  597.9 36.2 %all-gather.61.cloned.1.call-done = bf16[1,2048,256]{2,1,0:T(8,128)(2,1)} async-done(((bf16[1,256,256]{2,1,0:T(8,128)(2,1)}), bf16[1,2048,256]{2,1,0:T(8,128)(2,1)}) %all-gather.61.cloned.1.call-update) | async-done | bytes 1048592 | tf_op jit(solution)/shard_map/all_gather | solution.py:10
  638.9 36.2 %all-gather.59.cloned.1.call-done = bf16[1,2048,256]{2,1,0:T(8,128)(2,1)} async-done(((bf16[1,256,256]{2,1,0:T(8,128)(2,1)}), bf16[1,2048,256]{2,1,0:T(8,128)(2,1)}) %all-gather.59.cloned.1.call-update) | async-done | bytes 1048592 | tf_op jit(solution)/shard_map/all_gather | solution.py:10
  675.0 4.9 convolution_convert_fusion.2
  685.5 30.5 %all-gather.65.cloned.1.call-done = bf16[1,1024,512]{2,1,0:T(8,128)(2,1)} async-done(((bf16[1,128,512]{2,1,0:T(8,128)(2,1)}), bf16[1,1024,512]{2,1,0:T(8,128)(2,1)}) %all-gather.65.cloned.1.call-update) | async-done | bytes 1048592 | tf_op jit(solution)/shard_map/all_gather | solution.py:10
  716.0 29.1 %all-gather.41.cloned.1.call-done = bf16[6,256,1024]{2,1,0:T(8,128)(2,1)} async-done(((bf16[6,256,256]{2,1,0:T(8,128)(2,1)}), bf16[6,256,1024]{2,1,0:T(8,128)(2,1)}) %all-gather.41.cloned.1.call-update) | async-done | bytes 3145744 | tf_op jit(solution)/shard_map/all_gather | solution.py:90
  745.1 5.6 fusion.30
  (90 shorter events, 81.8 us)
Async XLA Ops:
  6.5 51.5 %all-gather.31.cloned.1.call-start = ((), (), s32[]{:S(2)}) async-start(), calls=%async_computation | async-start | bytes 7864320 | tf_op jit(solution)/shard_map/all_gather | solution.py:70
  7.3 93.2 %all-gather.47.cloned.1.call-start = ((), (), s32[]{:S(2)}) async-start(), calls=%async_computation.8 | async-start | bytes 1179648 | tf_op jit(solution)/shard_map/all_gather | solution.py:10
  8.3 133.3 %all-gather.45.cloned.1.call-start = ((), (), s32[]{:S(2)}) async-start(), calls=%async_computation.7 | async-start | bytes 1179648 | tf_op jit(solution)/shard_map/all_gather | solution.py:10
  9.1 173.5 %all-gather.43.cloned.1.call-start = ((), (), s32[]{:S(2)}) async-start(), calls=%async_computation.6 | async-start | bytes 1179648 | tf_op jit(solution)/shard_map/all_gather | solution.py:10
  10.0 213.6 %all-gather.49.cloned.1.call-start = ((), (), s32[]{:S(2)}) async-start(), calls=%async_computation.9 | async-start | bytes 1179648 | tf_op jit(solution)/shard_map/all_gather | solution.py:10
  10.8 241.8 %all-gather.33.cloned.1.call-start = ((), (), s32[]{:S(2)}) async-start(), calls=%async_computation.1 | async-start | bytes 3932160 | tf_op jit(solution)/shard_map/all_gather | solution.py:90
  58.0 4.6 copy-start
  187.7 3.9 collective-permute-start
  193.0 111.3 %all-gather.35.cloned.1.call-start = ((), (), s32[]{:S(2)}) async-start(), calls=%async_computation.2 | async-start | bytes 7864320 | tf_op jit(solution)/shard_map/all_gather | solution.py:70
  257.8 88.9 %all-gather.55.cloned.1.call-start = ((), (), s32[]{:S(2)}) async-start(), calls=%async_computation.12 | async-start | bytes 1179648 | tf_op jit(solution)/shard_map/all_gather | solution.py:10
  258.5 129.3 %all-gather.53.cloned.1.call-start = ((), (), s32[]{:S(2)}) async-start(), calls=%async_computation.11 | async-start | bytes 1179648 | tf_op jit(solution)/shard_map/all_gather | solution.py:10
  259.3 169.6 %all-gather.51.cloned.1.call-start = ((), (), s32[]{:S(2)}) async-start(), calls=%async_computation.10 | async-start | bytes 1179648 | tf_op jit(solution)/shard_map/all_gather | solution.py:10
  259.9 210.2 %all-gather.57.cloned.1.call-start = ((), (), s32[]{:S(2)}) async-start(), calls=%async_computation.13 | async-start | bytes 1179648 | tf_op jit(solution)/shard_map/all_gather | solution.py:10
  260.6 238.5 %all-gather.37.cloned.1.call-start = ((), (), s32[]{:S(2)}) async-start(), calls=%async_computation.3 | async-start | bytes 3932160 | tf_op jit(solution)/shard_map/all_gather | solution.py:90
  304.3 4.6 copy-start.2
  434.0 3.9 collective-permute-start.1
  439.4 111.4 %all-gather.39.cloned.1.call-start = ((), (), s32[]{:S(2)}) async-start(), calls=%async_computation.4 | async-start | bytes 7864320 | tf_op jit(solution)/shard_map/all_gather | solution.py:70
  504.2 88.8 %all-gather.63.cloned.1.call-start = ((), (), s32[]{:S(2)}) async-start(), calls=%async_computation.16 | async-start | bytes 1179648 | tf_op jit(solution)/shard_map/all_gather | solution.py:10
  504.8 129.2 %all-gather.61.cloned.1.call-start = ((), (), s32[]{:S(2)}) async-start(), calls=%async_computation.15 | async-start | bytes 1179648 | tf_op jit(solution)/shard_map/all_gather | solution.py:10
  505.4 169.6 %all-gather.59.cloned.1.call-start = ((), (), s32[]{:S(2)}) async-start(), calls=%async_computation.14 | async-start | bytes 1179648 | tf_op jit(solution)/shard_map/all_gather | solution.py:10
  506.0 210.1 %all-gather.65.cloned.1.call-start = ((), (), s32[]{:S(2)}) async-start(), calls=%async_computation.17 | async-start | bytes 1179648 | tf_op jit(solution)/shard_map/all_gather | solution.py:10
  506.6 238.5 %all-gather.41.cloned.1.call-start = ((), (), s32[]{:S(2)}) async-start(), calls=%async_computation.5 | async-start | bytes 3932160 | tf_op jit(solution)/shard_map/all_gather | solution.py:90
  550.8 4.6 copy-start.1
  680.1 3.9 collective-permute-start.2
  (6 other events, 13.5 us)
Sparse Core Ops, SparseCore 0:
  8.9 49.0 all-gather.30
  60.1 40.2 all-gather.46
  102.6 38.9 all-gather.44
  143.6 38.9 all-gather.42
  184.6 38.9 all-gather.48
  225.0 27.6 all-gather.32
  257.9 46.3 all-gather.34
  306.4 40.2 all-gather.54
  348.9 38.9 all-gather.52
  389.9 38.9 all-gather.50
  431.0 38.9 all-gather.56
  471.5 27.6 all-gather.36
  504.4 46.3 all-gather.38
  552.7 40.2 all-gather.62
  595.0 38.9 all-gather.60
  636.0 38.9 all-gather.58
  677.0 38.9 all-gather.64
  717.4 27.6 all-gather.40
where the time goes:
time: 758 us
  waiting for transfers between devices  641 us (85%)
  matrix products  59.6 us (8%)
  other arithmetic  30.2 us (4%)
  between operations  13.9 us (2%)
  starting transfers between devices  8.51 us (1%)
    all_gather x12, waiting for transfers between devices, taken_in(): lax.all_gather(part, axis, axis=dim, tiled=True)  410 us
    all_gather x3, waiting for transfers between devices, local(): whole = lax.all_gather(current, 'tp', axis=2, tiled=True)  134 us
    all_gather x3, waiting for transfers between devices, local(): full_mix = lax.all_gather(mixer, 'tp', axis=2, tiled=True)  87.2 us
    dot_general x9, matrix products, add_rows(): jnp.dot(columns, piece, preferred_element_type=jnp.float32)  43.7 us
    dot_general x3, matrix products, add_rows(): return total + jnp.dot(columns, piece, preferred_element_type=jnp.float32)  15.9 us
  transfers between devices with their start and end apart: 21, of which 21 were waited for; matrix products, arithmetic and copies ran while one was open for 10% of the time, Pallas kernels for 0%

commit v1 on v0

--- a/solution.py
+++ b/solution.py
@@ -1,9 +1,28 @@
+import functools
 import jax
 import jax.numpy as jnp
 from jax import lax
 from jax.sharding import PartitionSpec as P
 
 epsilon = 1e-06
+
+
+def _follow_slot(inp, a_name, join_dim):
+    n_shards = lax.axis_size(a_name)
+    later = [None] * n_shards
+    items = list(map(lambda ii: (ii, (ii + 1) % n_shards), range(n_shards)))
+    later[n_shards - 1] = inp
+    for j in range(n_shards - 2, -1, -1):
+        later[j] = lax.ppermute(later[j + 1], axis_name=a_name, perm=items)
+    e_now = jnp.roll(
+        jnp.concatenate(later, axis=join_dim),
+        (lax.axis_index(a_name) + 1) * inp.shape[join_dim],
+        axis=join_dim,
+    )
+    return e_now
+
+
+wrap_quotas_on_mesh = functools.partial(_follow_slot, a_name="tp", join_dim=2)
 
 
 def taken_in(array, axis, dim, take_in, carry):
@@ -87,7 +106,7 @@
         conved = convolve(extended, conv_taps[layer])
         mixer = (kept.astype(jnp.float32) * conved).astype(jnp.bfloat16)
         out_rows = mixer.shape[1]
-        full_mix = lax.all_gather(mixer, "tp", axis=2, tiled=True)
+        full_mix = wrap_quotas_on_mesh(mixer)
         flat_mix = full_mix.reshape(sequences * out_rows, full_mix.shape[2])
         projected = project_output(flat_mix, weight_output[layer])
         result = projected.reshape(sequences, out_rows, projected.shape[1])

time: 758 us -> 705 us (0.930)
  waiting for transfers between devices: 641 us -> 583 us
    all_gather x3 -> x0, waiting for transfers between devices: 87.2 us -> none  [local(): full_mix = lax.all_gather(mixer, 'tp', axis=2, tiled=True)]
    ppermute x0 -> x9, waiting for transfers between devices: none -> 67.5 us  [_follow_slot(): later[j] = lax.ppermute(later[j + 1], axis_name=a_name, perm=items)]
    all_gather x12, waiting for transfers between devices: 410 us -> 377 us  [taken_in(): lax.all_gather(part, axis, axis=dim, tiled=True)]
  transfers between devices with their start and end apart: 21 -> 27, of which waited for: 21 -> 24; matrix products, arithmetic and copies ran while one was open for 10% -> 9% of each run, Pallas kernels for 0% -> 0%
where the time goes in v1:
time: 705 us
  waiting for transfers between devices  583 us (83%)
  matrix products  63.9 us (9%)
  other arithmetic  27.6 us (4%)
  between operations  13.5 us (2%)
  starting transfers between devices  8.59 us (1%)
  local copies, waits for them, and re-layouts  8.12 us (1%)
    all_gather x12, waiting for transfers between devices, taken_in(): lax.all_gather(part, axis, axis=dim, tiled=True)  377 us
    all_gather x3, waiting for transfers between devices, local(): whole = lax.all_gather(current, 'tp', axis=2, tiled=True)  130 us
    ppermute x9, waiting for transfers between devices, _follow_slot(): later[j] = lax.ppermute(later[j + 1], axis_name=a_name, perm=items)  67.5 us
    dot_general x9, matrix products, add_rows(): jnp.dot(columns, piece, preferred_element_type=jnp.float32)  43.6 us
    dot_general x3, matrix products, add_rows(): return total + jnp.dot(columns, piece, preferred_element_type=jnp.float32)  20.3 us
  transfers between devices with their start and end apart: 27, of which 24 were waited for; matrix products, arithmetic and copies ran while one was open for 9% of the time, Pallas kernels for 0%

profile of v1, /device:TPU:0, one launch (start us, length us, event | category | flops | bytes accessed | tf_op | source)
XLA Modules:
  0.0 704.9 jit_solution(14110616902194250112)
XLA Ops:
  13.8 44.2 %all-gather.28.cloned.1.call-done = bf16[6,256,2048]{2,1,0:T(8,128)(2,1)} async-done(((bf16[6,256,512]{2,1,0:T(8,128)(2,1)}), bf16[6,256,2048]{2,1,0:T(8,128)(2,1)}) %all-gather.28.cloned.1.call-update) | async-done | bytes 6291472 | tf_op jit(solution)/shard_map/all_gather | solution.py:89
  66.8 33.7 %all-gather.38.cloned.1.call-done = bf16[1,2048,256]{2,1,0:T(8,128)(2,1)} async-done(((bf16[1,256,256]{2,1,0:T(8,128)(2,1)}), bf16[1,2048,256]{2,1,0:T(8,128)(2,1)}) %all-gather.38.cloned.1.call-update) | async-done | bytes 1048592 | tf_op jit(solution)/shard_map/all_gather | solution.py:29
  105.3 36.3 %all-gather.36.cloned.1.call-done = bf16[1,2048,256]{2,1,0:T(8,128)(2,1)} async-done(((bf16[1,256,256]{2,1,0:T(8,128)(2,1)}), bf16[1,2048,256]{2,1,0:T(8,128)(2,1)}) %all-gather.36.cloned.1.call-update) | async-done | bytes 1048592 | tf_op jit(solution)/shard_map/all_gather | solution.py:29
  146.5 36.1 %all-gather.34.cloned.1.call-done = bf16[1,2048,256]{2,1,0:T(8,128)(2,1)} async-done(((bf16[1,256,256]{2,1,0:T(8,128)(2,1)}), bf16[1,2048,256]{2,1,0:T(8,128)(2,1)}) %all-gather.34.cloned.1.call-update) | async-done | bytes 1048592 | tf_op jit(solution)/shard_map/all_gather | solution.py:29
  193.0 10.6 %collective-permute-done.1 = bf16[6,256,256]{2,1,0:T(8,128)(2,1)S(1)} collective-permute-done((bf16[6,256,256]{2,1,0:T(8,128)(2,1)S(1)}, bf16[6,256,256]{2,1,0:T(8,128)(2,1)S(1)}, u32[]{:S(2)}, u32[]{:S(2)}) %collective-permute-start.1) | collective-permute-done | bytes 786464 | tf_op jit(solution)/shard_map/ppermute | solution.py:16
  203.6 11.4 %collective-permute-done.2 = bf16[6,256,256]{2,1,0:T(8,128)(2,1)S(1)} collective-permute-done((bf16[6,256,256]{2,1,0:T(8,128)(2,1)S(1)}, bf16[6,256,256]{2,1,0:T(8,128)(2,1)S(1)}, u32[]{:S(2)}, u32[]{:S(2)}) %collective-permute-start.2) | collective-permute-done | bytes 786464 | tf_op jit(solution)/shard_map/ppermute | solution.py:16
  215.0 20.0 %all-gather.40.cloned.1.call-done = bf16[1,1024,512]{2,1,0:T(8,128)(2,1)} async-done(((bf16[1,128,512]{2,1,0:T(8,128)(2,1)}), bf16[1,1024,512]{2,1,0:T(8,128)(2,1)}) %all-gather.40.cloned.1.call-update) | async-done | bytes 1048592 | tf_op jit(solution)/shard_map/all_gather | solution.py:29
  235.0 6.8 fusion.39
  244.3 42.8 %all-gather.30.cloned.1.call-done = bf16[6,256,2048]{2,1,0:T(8,128)(2,1)} async-done(((bf16[6,256,512]{2,1,0:T(8,128)(2,1)}), bf16[6,256,2048]{2,1,0:T(8,128)(2,1)}) %all-gather.30.cloned.1.call-update) | async-done | bytes 6291472 | tf_op jit(solution)/shard_map/all_gather | solution.py:89
  295.8 33.7 %all-gather.46.cloned.1.call-done = bf16[1,2048,256]{2,1,0:T(8,128)(2,1)} async-done(((bf16[1,256,256]{2,1,0:T(8,128)(2,1)}), bf16[1,2048,256]{2,1,0:T(8,128)(2,1)}) %all-gather.46.cloned.1.call-update) | async-done | bytes 1048592 | tf_op jit(solution)/shard_map/all_gather | solution.py:29
  334.3 36.3 %all-gather.44.cloned.1.call-done = bf16[1,2048,256]{2,1,0:T(8,128)(2,1)} async-done(((bf16[1,256,256]{2,1,0:T(8,128)(2,1)}), bf16[1,2048,256]{2,1,0:T(8,128)(2,1)}) %all-gather.44.cloned.1.call-update) | async-done | bytes 1048592 | tf_op jit(solution)/shard_map/all_gather | solution.py:29
  375.5 36.3 %all-gather.42.cloned.1.call-done = bf16[1,2048,256]{2,1,0:T(8,128)(2,1)} async-done(((bf16[1,256,256]{2,1,0:T(8,128)(2,1)}), bf16[1,2048,256]{2,1,0:T(8,128)(2,1)}) %all-gather.42.cloned.1.call-update) | async-done | bytes 1048592 | tf_op jit(solution)/shard_map/all_gather | solution.py:29
  421.4 11.3 %collective-permute-done.5 = bf16[6,256,256]{2,1,0:T(8,128)(2,1)S(1)} collective-permute-done((bf16[6,256,256]{2,1,0:T(8,128)(2,1)S(1)}, bf16[6,256,256]{2,1,0:T(8,128)(2,1)S(1)}, u32[]{:S(2)}, u32[]{:S(2)}) %collective-permute-start.5) | collective-permute-done | bytes 786464 | tf_op jit(solution)/shard_map/ppermute | solution.py:16
  432.8 11.4 %collective-permute-done.6 = bf16[6,256,256]{2,1,0:T(8,128)(2,1)S(1)} collective-permute-done((bf16[6,256,256]{2,1,0:T(8,128)(2,1)S(1)}, bf16[6,256,256]{2,1,0:T(8,128)(2,1)S(1)}, u32[]{:S(2)}, u32[]{:S(2)}) %collective-permute-start.6) | collective-permute-done | bytes 786464 | tf_op jit(solution)/shard_map/ppermute | solution.py:16
  444.2 19.3 %all-gather.48.cloned.1.call-done = bf16[1,1024,512]{2,1,0:T(8,128)(2,1)} async-done(((bf16[1,128,512]{2,1,0:T(8,128)(2,1)}), bf16[1,1024,512]{2,1,0:T(8,128)(2,1)}) %all-gather.48.cloned.1.call-update) | async-done | bytes 1048592 | tf_op jit(solution)/shard_map/all_gather | solution.py:29
  463.5 6.8 fusion.36
  472.4 43.0 %all-gather.32.cloned.1.call-done = bf16[6,256,2048]{2,1,0:T(8,128)(2,1)} async-done(((bf16[6,256,512]{2,1,0:T(8,128)(2,1)}), bf16[6,256,2048]{2,1,0:T(8,128)(2,1)}) %all-gather.32.cloned.1.call-update) | async-done | bytes 6291472 | tf_op jit(solution)/shard_map/all_gather | solution.py:89
  524.2 33.5 %all-gather.54.cloned.1.call-done = bf16[1,2048,256]{2,1,0:T(8,128)(2,1)} async-done(((bf16[1,256,256]{2,1,0:T(8,128)(2,1)}), bf16[1,2048,256]{2,1,0:T(8,128)(2,1)}) %all-gather.54.cloned.1.call-update) | async-done | bytes 1048592 | tf_op jit(solution)/shard_map/all_gather | solution.py:29
  562.6 36.3 %all-gather.52.cloned.1.call-done = bf16[1,2048,256]{2,1,0:T(8,128)(2,1)} async-done(((bf16[1,256,256]{2,1,0:T(8,128)(2,1)}), bf16[1,2048,256]{2,1,0:T(8,128)(2,1)}) %all-gather.52.cloned.1.call-update) | async-done | bytes 1048592 | tf_op jit(solution)/shard_map/all_gather | solution.py:29
  603.8 36.1 %all-gather.50.cloned.1.call-done = bf16[1,2048,256]{2,1,0:T(8,128)(2,1)} async-done(((bf16[1,256,256]{2,1,0:T(8,128)(2,1)}), bf16[1,2048,256]{2,1,0:T(8,128)(2,1)}) %all-gather.50.cloned.1.call-update) | async-done | bytes 1048592 | tf_op jit(solution)/shard_map/all_gather | solution.py:29
  649.5 11.4 %collective-permute-done.9 = bf16[6,256,256]{2,1,0:T(8,128)(2,1)S(1)} collective-permute-done((bf16[6,256,256]{2,1,0:T(8,128)(2,1)S(1)}, bf16[6,256,256]{2,1,0:T(8,128)(2,1)S(1)}, u32[]{:S(2)}, u32[]{:S(2)}) %collective-permute-start.9) | collective-permute-done | bytes 786464 | tf_op jit(solution)/shard_map/ppermute | solution.py:16
  660.9 11.4 %collective-permute-done.10 = bf16[6,256,256]{2,1,0:T(8,128)(2,1)S(1)} collective-permute-done((bf16[6,256,256]{2,1,0:T(8,128)(2,1)S(1)}, bf16[6,256,256]{2,1,0:T(8,128)(2,1)S(1)}, u32[]{:S(2)}, u32[]{:S(2)}) %collective-permute-start.10) | collective-permute-done | bytes 786464 | tf_op jit(solution)/shard_map/ppermute | solution.py:16
  672.3 19.3 %all-gather.56.cloned.1.call-done = bf16[1,1024,512]{2,1,0:T(8,128)(2,1)} async-done(((bf16[1,128,512]{2,1,0:T(8,128)(2,1)}), bf16[1,1024,512]{2,1,0:T(8,128)(2,1)}) %all-gather.56.cloned.1.call-update) | async-done | bytes 1048592 | tf_op jit(solution)/shard_map/all_gather | solution.py:29
  691.6 6.7 fusion.34
  (91 shorter events, 96.7 us)
Async XLA Ops:
  6.5 51.5 %all-gather.28.cloned.1.call-start = ((), (), s32[]{:S(2)}) async-start(), calls=%async_computation | async-start | bytes 7864320 | tf_op jit(solution)/shard_map/all_gather | solution.py:89
  7.3 93.2 %all-gather.38.cloned.1.call-start = ((), (), s32[]{:S(2)}) async-start(), calls=%async_computation.5 | async-start | bytes 1179648 | tf_op jit(solution)/shard_map/all_gather | solution.py:29
  9.1 132.5 %all-gather.36.cloned.1.call-start = ((), (), s32[]{:S(2)}) async-start(), calls=%async_computation.4 | async-start | bytes 1179648 | tf_op jit(solution)/shard_map/all_gather | solution.py:29
  11.0 171.6 %all-gather.34.cloned.1.call-start = ((), (), s32[]{:S(2)}) async-start(), calls=%async_computation.3 | async-start | bytes 1179648 | tf_op jit(solution)/shard_map/all_gather | solution.py:29
  12.8 222.2 %all-gather.40.cloned.1.call-start = ((), (), s32[]{:S(2)}) async-start(), calls=%async_computation.6 | async-start | bytes 1179648 | tf_op jit(solution)/shard_map/all_gather | solution.py:29
  192.1 11.5 %collective-permute-start.1 = (bf16[6,256,256]{2,1,0:T(8,128)(2,1)S(1)}, bf16[6,256,256]{2,1,0:T(8,128)(2,1)S(1)}, u32[]{:S(2)}, u32[]{:S(2)}) collective-permute-start(bf16[6,256,256]{2,1,0:T(8,128)(2,1)S(1)} %fusion.59), channel_id=1, source_target_pairs={{0,1},{1,2},{2,3},{3,0},{4,5},{5,6},{6,7},{7,4},{8,9},{9,10},{10,1... | collective-permute-start | bytes 2359304 | tf_op jit(solution)/shard_map/ppermute | solution.py:16
  193.0 94.1 %all-gather.30.cloned.1.call-start = ((), (), s32[]{:S(2)}) async-start(), calls=%async_computation.1 | async-start | bytes 7864320 | tf_op jit(solution)/shard_map/all_gather | solution.py:89
  203.6 11.4 %collective-permute-start.2 = (bf16[6,256,256]{2,1,0:T(8,128)(2,1)S(1)}, bf16[6,256,256]{2,1,0:T(8,128)(2,1)S(1)}, u32[]{:S(2)}, u32[]{:S(2)}) collective-permute-start(bf16[6,256,256]{2,1,0:T(8,128)(2,1)S(1)} %collective-permute-done.1), channel_id=1, source_target_pairs={{0,1},{1,2},{2,3},{3,0},{4,5},{5,6},{6,7},{7,4},{8,9},{9,10},{10,1... | collective-permute-start | bytes 2359304 | tf_op jit(solution)/shard_map/ppermute | solution.py:16
  215.0 20.0 %collective-permute-start.3 = (bf16[6,256,256]{2,1,0:T(8,128)(2,1)S(1)}, bf16[6,256,256]{2,1,0:T(8,128)(2,1)S(1)}, u32[]{:S(2)}, u32[]{:S(2)}) collective-permute-start(bf16[6,256,256]{2,1,0:T(8,128)(2,1)S(1)} %collective-permute-done.2), channel_id=1, source_target_pairs={{0,1},{1,2},{2,3},{3,0},{4,5},{5,6},{6,7},{7,4},{8,9},{9,10},{10,1... | collective-permute-start | bytes 2359304 | tf_op jit(solution)/shard_map/ppermute | solution.py:16
  241.8 87.7 %all-gather.46.cloned.1.call-start = ((), (), s32[]{:S(2)}) async-start(), calls=%async_computation.9 | async-start | bytes 1179648 | tf_op jit(solution)/shard_map/all_gather | solution.py:29
  242.6 128.1 %all-gather.44.cloned.1.call-start = ((), (), s32[]{:S(2)}) async-start(), calls=%async_computation.8 | async-start | bytes 1179648 | tf_op jit(solution)/shard_map/all_gather | solution.py:29
  243.3 168.5 %all-gather.42.cloned.1.call-start = ((), (), s32[]{:S(2)}) async-start(), calls=%async_computation.7 | async-start | bytes 1179648 | tf_op jit(solution)/shard_map/all_gather | solution.py:29
  244.0 219.4 %all-gather.48.cloned.1.call-start = ((), (), s32[]{:S(2)}) async-start(), calls=%async_computation.10 | async-start | bytes 1179648 | tf_op jit(solution)/shard_map/all_gather | solution.py:29
  421.3 11.5 %collective-permute-start.5 = (bf16[6,256,256]{2,1,0:T(8,128)(2,1)S(1)}, bf16[6,256,256]{2,1,0:T(8,128)(2,1)S(1)}, u32[]{:S(2)}, u32[]{:S(2)}) collective-permute-start(bf16[6,256,256]{2,1,0:T(8,128)(2,1)S(1)} %fusion.53), channel_id=1, source_target_pairs={{0,1},{1,2},{2,3},{3,0},{4,5},{5,6},{6,7},{7,4},{8,9},{9,10},{10,1... | collective-permute-start | bytes 2359304 | tf_op jit(solution)/shard_map/ppermute | solution.py:16
  421.4 94.1 %all-gather.32.cloned.1.call-start = ((), (), s32[]{:S(2)}) async-start(), calls=%async_computation.2 | async-start | bytes 7864320 | tf_op jit(solution)/shard_map/all_gather | solution.py:89
  432.8 11.4 %collective-permute-start.6 = (bf16[6,256,256]{2,1,0:T(8,128)(2,1)S(1)}, bf16[6,256,256]{2,1,0:T(8,128)(2,1)S(1)}, u32[]{:S(2)}, u32[]{:S(2)}) collective-permute-start(bf16[6,256,256]{2,1,0:T(8,128)(2,1)S(1)} %collective-permute-done.5), channel_id=1, source_target_pairs={{0,1},{1,2},{2,3},{3,0},{4,5},{5,6},{6,7},{7,4},{8,9},{9,10},{10,1... | collective-permute-start | bytes 2359304 | tf_op jit(solution)/shard_map/ppermute | solution.py:16
  444.2 19.3 %collective-permute-start.7 = (bf16[6,256,256]{2,1,0:T(8,128)(2,1)S(1)}, bf16[6,256,256]{2,1,0:T(8,128)(2,1)S(1)}, u32[]{:S(2)}, u32[]{:S(2)}) collective-permute-start(bf16[6,256,256]{2,1,0:T(8,128)(2,1)S(1)} %collective-permute-done.6), channel_id=1, source_target_pairs={{0,1},{1,2},{2,3},{3,0},{4,5},{5,6},{6,7},{7,4},{8,9},{9,10},{10,1... | collective-permute-start | bytes 2359304 | tf_op jit(solution)/shard_map/ppermute | solution.py:16
  470.3 87.5 %all-gather.54.cloned.1.call-start = ((), (), s32[]{:S(2)}) async-start(), calls=%async_computation.13 | async-start | bytes 1179648 | tf_op jit(solution)/shard_map/all_gather | solution.py:29
  470.8 128.1 %all-gather.52.cloned.1.call-start = ((), (), s32[]{:S(2)}) async-start(), calls=%async_computation.12 | async-start | bytes 1179648 | tf_op jit(solution)/shard_map/all_gather | solution.py:29
  471.6 168.3 %all-gather.50.cloned.1.call-start = ((), (), s32[]{:S(2)}) async-start(), calls=%async_computation.11 | async-start | bytes 1179648 | tf_op jit(solution)/shard_map/all_gather | solution.py:29
  472.2 219.4 %all-gather.56.cloned.1.call-start = ((), (), s32[]{:S(2)}) async-start(), calls=%async_computation.14 | async-start | bytes 1179648 | tf_op jit(solution)/shard_map/all_gather | solution.py:29
  649.4 11.5 %collective-permute-start.9 = (bf16[6,256,256]{2,1,0:T(8,128)(2,1)S(1)}, bf16[6,256,256]{2,1,0:T(8,128)(2,1)S(1)}, u32[]{:S(2)}, u32[]{:S(2)}) collective-permute-start(bf16[6,256,256]{2,1,0:T(8,128)(2,1)S(1)} %fusion.47), channel_id=1, source_target_pairs={{0,1},{1,2},{2,3},{3,0},{4,5},{5,6},{6,7},{7,4},{8,9},{9,10},{10,1... | collective-permute-start | bytes 2359304 | tf_op jit(solution)/shard_map/ppermute | solution.py:16
  660.9 11.4 %collective-permute-start.10 = (bf16[6,256,256]{2,1,0:T(8,128)(2,1)S(1)}, bf16[6,256,256]{2,1,0:T(8,128)(2,1)S(1)}, u32[]{:S(2)}, u32[]{:S(2)}) collective-permute-start(bf16[6,256,256]{2,1,0:T(8,128)(2,1)S(1)} %collective-permute-done.9), channel_id=1, source_target_pairs={{0,1},{1,2},{2,3},{3,0},{4,5},{5,6},{6,7},{7,4},{8,9},{9,10},{10,1... | collective-permute-start | bytes 2359304 | tf_op jit(solution)/shard_map/ppermute | solution.py:16
  672.3 19.3 %collective-permute-start.11 = (bf16[6,256,256]{2,1,0:T(8,128)(2,1)S(1)}, bf16[6,256,256]{2,1,0:T(8,128)(2,1)S(1)}, u32[]{:S(2)}, u32[]{:S(2)}) collective-permute-start(bf16[6,256,256]{2,1,0:T(8,128)(2,1)S(1)} %collective-permute-done.10), channel_id=1, source_target_pairs={{0,1},{1,2},{2,3},{3,0},{4,5},{5,6},{6,7},{7,4},{8,9},{9,10},{10,1... | collective-permute-start | bytes 2359304 | tf_op jit(solution)/shard_map/ppermute | solution.py:16
  (8 other events, 73.8 us)
Sparse Core Ops, SparseCore 0:
  8.9 49.0 all-gather.27
  60.1 40.2 all-gather.37
  102.6 38.9 all-gather.35
  143.6 38.9 all-gather.33
  193.1 41.8 all-gather.39
  241.9 45.0 all-gather.29
  289.2 40.2 all-gather.45
  331.6 38.9 all-gather.43
  372.7 38.9 all-gather.41
  421.5 41.9 all-gather.47
  470.4 45.0 all-gather.31
  517.5 40.2 all-gather.53
  559.9 38.9 all-gather.51
  600.9 38.9 all-gather.49
  649.7 41.9 all-gather.55
